TPU v7x, 32 devices: a whole 2x2x4 slice. The times are simulated.
32 devices in a mesh: sp: 16 (over z, y, x), tp: 2 (over core).
Axes of the slice: x: 2, y: 2, z: 4, core: 2. Of those that a mesh axis runs over, the one named last changes fastest.
Arguments:
- stream: bfloat16 [2048, 2048], P(('sp', 'tp')), may hold values from -6 to 6
- wide_head_query: bfloat16 [2048, 1024], P('sp', 'tp'), may hold values from -6 to 6
- broad_attention_lookup_vectors: bfloat16 [2048, 1024], P('sp', 'tp'), may hold values from -6 to 6
- values_wide: bfloat16 [2048, 2048], P('sp', 'tp'), may hold values from -6 to 6
- query_narrow: bfloat16 [2048, 512], P('sp', 'tp'), may hold values from -6 to 6
- keys_narrow: bfloat16 [2048, 512], P('sp', 'tp'), may hold values from -6 to 6
- values_narrow: bfloat16 [2048, 1024], P('sp', 'tp'), may hold values from -6 to 6
- gate_wide: bfloat16 [2048, 2048], P('sp', 'tp'), may hold values from -6 to 6
- gate_narrow: bfloat16 [2048, 1024], P('sp', 'tp'), may hold values from -6 to 6
- log_decay: float32 [2, 8, 2048], P(None, 'tp', 'sp'), may hold values from -1.2 to 0, as said below
- gain_wide: bfloat16 [2048], P('tp'), may hold values from 0.099609375 to 1.8984375
- gain_narrow: bfloat16 [1024], P('tp'), may hold values from 0.099609375 to 1.8984375
- out_wide: bfloat16 [2048, 2048], P('tp'), may hold values from -0.109375 to 0.109375
- out_narrow: bfloat16 [1024, 2048], P('tp'), may hold values from -0.109375 to 0.109375
- gain_mix: bfloat16 [2048], replicated, may hold values from 0.099609375 to 1.8984375
- gain_pre: bfloat16 [2048], replicated, may hold values from 0.099609375 to 1.8984375
- gain_post: bfloat16 [2048], replicated, may hold values from 0.099609375 to 1.8984375
- weight_gate: bfloat16 [2048, 5120], P('sp', 'tp'), may hold values from -0.125 to 0.125
- weight_lin: bfloat16 [2048, 5120], P('sp', 'tp'), may hold values from -0.125 to 0.125
- weight_down: bfloat16 [2048, 5120], P('sp', 'tp'), may hold values from -0.078125 to 0.078125
- taps_gate: bfloat16 [3, 5120], P(None, 'tp'), may hold values from -3 to 3
- taps_lin: bfloat16 [3, 5120], P(None, 'tp'), may hold values from -3 to 3
Outputs:
- stream_out: bfloat16 [2048, 2048], P(('sp', 'tp'))
Inputs may be any that keep to these rules, and one draw needn't show every extreme that they name: `log_decay`: the natural logarithm of the factor by which one head's retained state is multiplied at one position.
All inputs are finite; a program needn't handle non-finite values.
Results may differ from a plain program's by a relative error of at most 0.023.
Values may be sent and summed in bfloat16 or wider, within the bound.
A program may use at most 128 MiB of HBM per device.

v0:
```python
import jax
import jax.numpy as jnp
from jax import lax
from jax.sharding import PartitionSpec as P

KW = 128
VW = 256
KN = 64
VN = 128
BLOCK = 128


EPS = 1e-06
THETA = 10000.0


def carried_in(x, axis, join, neutral):
    place = lax.axis_index(axis)
    gathered = jax.tree.map(
        lambda a, kind: lax.all_gather(a.astype(kind), axis),
        x,
        (jnp.bfloat16, jnp.bfloat16, jnp.bfloat16, jnp.bfloat16),
    )
    state = jax.tree.map(lambda a, e: jnp.zeros_like(a) + jnp.asarray(e, a.dtype), x, neutral)

    def one(lap, state):
        return join(
            state,
            jax.tree.map(
                lambda a, own: lax.dynamic_index_in_dim(a, lap, 0, False).astype(own.dtype),
                gathered,
                x,
            ),
        )

    return lax.fori_loop(0, place, one, state)


def passed_along(value, axis, steps):
    count = lax.axis_size(axis)
    first, last = (max(0, -steps), min(count, count - steps))
    return lax.ppermute(value, axis, [(source, source + steps) for source in range(first, last)])


def rotate(block, positions):
    width = block.shape[-1]
    half = width // 2
    frequency = THETA ** (-(jnp.arange(half, dtype=jnp.float32) * 2.0 / width))
    angles = positions.astype(jnp.float32)[:, None] * frequency[None, :]
    cosine = jnp.cos(angles)[:, None, :]
    sine = jnp.sin(angles)[:, None, :]
    values = block.astype(jnp.float32)
    first = values[..., :half]
    second = values[..., half:]
    return jnp.concatenate(
        [first * cosine - second * sine, second * cosine + first * sine], axis=-1
    )


def block_step(state, inputs):
    query, keys, values, log_rate = inputs
    running = jnp.cumsum(log_rate, axis=1)
    length = running.shape[1]
    index = jnp.arange(length)
    lower = (index[:, None] >= index[None, :])[None]
    spread = jnp.where(
        lower, jnp.exp(jnp.where(lower, running[:, :, None] - running[:, None, :], 0.0)), 0.0
    )
    scores = (
        jnp.einsum("ihd,jhd->hij", query, keys, preferred_element_type=jnp.float32) * spread
    ).astype(jnp.bfloat16)
    inner = jnp.einsum("hij,jhe->ihe", scores, values, preferred_element_type=jnp.float32)
    lifted = query.astype(jnp.float32) * jnp.exp(running).T[:, :, None]
    cross = jnp.einsum("ihd,hde->ihe", lifted, state, precision=lax.Precision.HIGHEST)
    tail = running[:, -1:]
    scaled = (keys.astype(jnp.float32) * jnp.exp(tail - running).T[:, :, None]).astype(jnp.bfloat16)
    update = jnp.einsum("jhd,jhe->hde", scaled, values, preferred_element_type=jnp.float32)
    state = state * jnp.exp(tail)[:, :, None] + update
    return (state, inner + cross)


def kept_nearby_memory(query, keys, values, log_rate, head_dim, value_dim, offset):
    rows = query.shape[0]
    heads = query.shape[1] // head_dim
    positions = offset + jnp.arange(rows, dtype=jnp.int32)
    rotated_query = rotate(query.reshape(rows, heads, head_dim), positions).astype(jnp.bfloat16)
    rotated_keys = (
        rotate(keys.reshape(rows, heads, head_dim), positions) * head_dim ** (-0.5)
    ).astype(jnp.bfloat16)
    layer_groups_list = rows // BLOCK

    def split(array):
        return array.reshape(layer_groups_list, BLOCK, heads, array.shape[-1])

    rates = jnp.transpose(log_rate.reshape(heads, layer_groups_list, BLOCK), (1, 0, 2))
    start = jnp.zeros((heads, head_dim, value_dim), jnp.float32)
    inputs = (
        split(rotated_query),
        split(rotated_keys),
        split(values.reshape(rows, heads, value_dim)),
        rates,
    )
    state, outs = lax.scan(block_step, start, inputs)
    return (rotated_query, outs.reshape(rows, heads, value_dim), state)


def carried(rotated_query, log_rate, state_in):
    lifted = rotated_query.astype(jnp.float32) * jnp.exp(jnp.cumsum(log_rate, axis=1)).T[:, :, None]
    return jnp.einsum("ihd,hde->ihe", lifted, state_in, precision=lax.Precision.HIGHEST)


def gate_heads(retained, gain, gate):
    mean = jnp.mean(retained, axis=-1, keepdims=True)
    centred = retained - mean
    variance = jnp.mean(centred * centred, axis=-1, keepdims=True)
    normed = (centred * lax.rsqrt(variance + EPS)).reshape(retained.shape[0], -1)
    return (normed * gain.astype(jnp.float32) * jax.nn.silu(gate.astype(jnp.float32))).astype(
        jnp.bfloat16
    )


def scale_rows(rows, gain):
    return (
        rows
        * lax.rsqrt(jnp.mean(rows * rows, axis=-1, keepdims=True) + EPS)
        * gain.astype(jnp.float32)
    )


def causal_taps(upward, before, taps):
    width = taps.shape[0]
    total = upward.shape[0]
    padded_rows = jnp.concatenate([before, upward], axis=0).astype(jnp.float32)
    smooth = jnp.zeros((total, upward.shape[1]), jnp.float32)
    for tap_index in range(width):
        smooth = (
            smooth
            + taps[tap_index].astype(jnp.float32)[None, :]
            * padded_rows[tap_index : tap_index + total]
        )
    return smooth


def chain(earlier, later):
    return (
        earlier[0] * later[2] + later[0],
        earlier[1] * later[3] + later[1],
        earlier[2] * later[2],
        earlier[3] * later[3],
    )


def body(
    stream,
    wide_head_query,
    broad_attention_lookup_vectors,
    values_wide,
    query_narrow,
    keys_narrow,
    values_narrow,
    gate_wide,
    gate_narrow,
    log_decay,
    gain_wide,
    gain_narrow,
    out_wide,
    out_narrow,
    gain_mix,
    gain_pre,
    gain_post,
    weight_gate,
    weight_lin,
    weight_down,
    taps_gate,
    taps_lin,
):
    rows = wide_head_query.shape[0]
    offset = lax.axis_index("sp") * rows
    rates_wide = log_decay[0]
    rates_narrow = log_decay[1]
    rot_wide, local_wide, state_wide = kept_nearby_memory(
        wide_head_query, broad_attention_lookup_vectors, values_wide, rates_wide, KW, VW, offset
    )
    rot_narrow, local_narrow, state_narrow = kept_nearby_memory(
        query_narrow, keys_narrow, values_narrow, rates_narrow, KN, VN, offset
    )
    decay_wide = jnp.exp(jnp.sum(rates_wide, axis=1))[:, None, None]
    decay_narrow = jnp.exp(jnp.sum(rates_narrow, axis=1))[:, None, None]
    identity = (
        jnp.zeros_like(state_wide),
        jnp.zeros_like(state_narrow),
        jnp.ones_like(decay_wide),
        jnp.ones_like(decay_narrow),
    )
    incoming = carried_in(
        (state_wide, state_narrow, decay_wide, decay_narrow), "sp", chain, identity
    )
    gated_wide = gate_heads(
        local_wide + carried(rot_wide, rates_wide, incoming[0]), gain_wide, gate_wide
    )
    gated_narrow = gate_heads(
        local_narrow + carried(rot_narrow, rates_narrow, incoming[1]), gain_narrow, gate_narrow
    )
    part_wide = jnp.dot(gated_wide, out_wide, preferred_element_type=jnp.float32)
    part_narrow = jnp.dot(gated_narrow, out_narrow, preferred_element_type=jnp.float32)
    mixed = lax.psum_scatter(
        (part_wide + part_narrow).astype(jnp.bfloat16), "tp", scatter_dimension=0, tiled=True
    ).astype(jnp.float32)
    resid = (stream.astype(jnp.float32) + scale_rows(mixed, gain_mix)).astype(jnp.bfloat16)
    normed_in = scale_rows(resid.astype(jnp.float32), gain_pre).astype(jnp.bfloat16)
    normed_all = lax.all_gather(normed_in, "tp", axis=0, tiled=True)
    whole_gate, whole_lin = (
        lax.all_gather(weight_gate, "sp", axis=0, tiled=True),
        lax.all_gather(weight_lin, "sp", axis=0, tiled=True),
    )
    up_gate = jnp.dot(normed_all, whole_gate, preferred_element_type=jnp.float32).astype(
        jnp.bfloat16
    )
    up_lin = jnp.dot(normed_all, whole_lin, preferred_element_type=jnp.float32).astype(jnp.bfloat16)
    reach = taps_gate.shape[0] - 1
    before_gate, before_lin = passed_along(
        (up_gate[rows - reach :], up_lin[rows - reach :]), "sp", 1
    )
    smooth_gate = causal_taps(up_gate, before_gate, taps_gate)
    smooth_lin = causal_taps(up_lin, before_lin, taps_lin)
    hidden = (jax.nn.silu(smooth_gate) * smooth_lin).astype(jnp.bfloat16)
    terms = lax.dot_general(
        hidden,
        lax.all_gather(weight_down, "sp", axis=0, tiled=True),
        (((1,), (1,)), ((), ())),
        preferred_element_type=jnp.float32,
    )
    fed = lax.psum_scatter(
        terms.astype(jnp.bfloat16), "tp", scatter_dimension=0, tiled=True
    ).astype(jnp.float32)
    return (resid.astype(jnp.float32) + scale_rows(fed, gain_post)).astype(jnp.bfloat16)


def solution(mesh):
    in_specs = (
        P(("sp", "tp"), None),
        P("sp", "tp"),
        P("sp", "tp"),
        P("sp", "tp"),
        P("sp", "tp"),
        P("sp", "tp"),
        P("sp", "tp"),
        P("sp", "tp"),
        P("sp", "tp"),
        P(None, "tp", "sp"),
        P("tp"),
        P("tp"),
        P("tp", None),
        P("tp", None),
        P(),
        P(),
        P(),
        P("sp", "tp"),
        P("sp", "tp"),
        P("sp", "tp"),
        P(None, "tp"),
        P(None, "tp"),
    )
    out_specs = P(("sp", "tp"), None)
    return jax.shard_map(body, mesh=mesh, in_specs=in_specs, out_specs=out_specs, check_vma=False)
```

profile of v0, /device:TPU:0, one launch (start us, length us, event | category | flops | bytes accessed | tf_op | source)
XLA Modules:
  0.0 636.4 jit_solution(3645589715548964104)
XLA Ops:
  6.6 1.0 slice_reduce_fusion.1
  7.6 1.0 copy.90
  8.6 1.0 copy.98
  11.0 1.0 copy.110
  16.9 1.1 subtract_convert_fusion
  18.8 1.1 fusion.13
  21.7 43.7 %all-reduce.2 = (bf16[64]{0:T(256)(128)(2,1)S(1)}, bf16[64]{0:T(256)(128)(2,1)S(1)}) all-reduce(bf16[64]{0:T(256)(128)(2,1)S(1)} %dynamic-update-slice, bf16[64]{0:T(256)(128)(2,1)S(1)} %dynamic-update-slice.1), channel_id=2, replica_groups=mesh['sp'=16,'tp'=2] {'sp'}, use_global_device_ids=true, to_apply=%add | all-reduce | flops 128 | bytes 512
  69.3 1.0 fusion.15
  70.3 1.9 convolution_bitcast_fusion.1
  72.4 77.2 %all-gather.16.cloned.1.call-done = bf16[64,128,256]{2,1,0:T(8,128)(2,1)} async-done(((bf16[4,128,256]{2,1,0:T(8,128)(2,1)}), bf16[64,128,256]{2,1,0:T(8,128)(2,1)}) %all-gather.16.cloned.1.call-update) | async-done | bytes 4194320 | tf_op jit(solution)/shard_map/all_gather | solution.py:20
  151.9 1.4 convolution_bitcast_fusion
  153.3 2.2 fusion.102
  156.8 1.2 fusion.41
  158.0 3.0 fusion.104
  161.1 1.3 fusion.4
  165.0 44.7 %reduce-scatter.3.cloned.1.call-done = bf16[64,2048]{1,0:T(8,128)(2,1)} async-done(((bf16[128,2048]{1,0:T(8,128)(2,1)}), bf16[64,2048]{1,0:T(8,128)(2,1)}) %reduce-scatter.3.cloned.1.call-update) | async-done | bytes 262160 | tf_op jit(solution)/shard_map/reduce_scatter | solution.py:206
  209.8 1.1 fusion.31
  210.9 1.3 fusion.37
  212.3 2.2 all_gather.38
  214.5 130.4 %all-gather.10.cloned.1.call-done = bf16[2048,2560]{1,0:T(8,128)(2,1)} async-done(((bf16[128,2560]{1,0:T(8,128)(2,1)}), bf16[2048,2560]{1,0:T(8,128)(2,1)}) %all-gather.10.cloned.1.call-update) | async-done | bytes 10485776 | tf_op jit(solution)/shard_map/all_gather | solution.py:213
  344.9 5.5 convolution_convert_fusion.1
  351.1 3.9 collective-permute-start
  355.0 122.2 %all-gather.12.cloned.1.call-done = bf16[2048,2560]{1,0:T(8,128)(2,1)} async-done(((bf16[128,2560]{1,0:T(8,128)(2,1)}), bf16[2048,2560]{1,0:T(8,128)(2,1)}) %all-gather.12.cloned.1.call-update) | async-done | bytes 10485776 | tf_op jit(solution)/shard_map/all_gather | solution.py:214
  477.2 5.5 convolution_convert_fusion
  482.7 3.4 collective-permute-start.1
  486.1 2.0 maximum_convert_fusion
  488.1 1.3 maximum_convert_fusion.1
  489.5 119.9 %all-gather.14.cloned.1.call-done = bf16[2048,2560]{1,0:T(8,128)(2,1)} async-done(((bf16[128,2560]{1,0:T(8,128)(2,1)}), bf16[2048,2560]{1,0:T(8,128)(2,1)}) %all-gather.14.cloned.1.call-update) | async-done | bytes 10485776 | tf_op jit(solution)/shard_map/all_gather | solution.py:229
  609.4 10.9 %convolution_convert_fusion.2 = bf16[128,2048]{1,0:T(8,128)(2,1)} fusion(bf16[2048,2560]{1,0:T(8,128)(2,1)} %all-gather.14.cloned.1.call-done, f32[130,2560]{1,0:T(8,128)} %maximum_convert_fusion.1, f32[130,2560]{1,0:T(8,128)} %maximum_convert_fusion, f32[2560]{0:T(1024)S(1)} %copy-done.23, f32[2560]{0:T(1024)S(1)} %copy-done.24, ...), kind=kOutput, calls=%fused_computation.12 | convolution fusion | flops 1347682304 | bytes 18935808 | tf_op jit(solution)/shard_map/dot_general | solution.py:227
  620.4 6.2 reduce-scatter.5.cloned.1.call-done
  626.7 1.1 fusion.35
  627.8 1.8 fusion.40
  (148 shorter events, 19.0 us)
Async XLA Ops:
  6.5 154.5 %copy-start = (bf16[512,2048]{1,0:T(8,128)(2,1)S(1)}, bf16[512,2048]{1,0:T(8,128)(2,1)}, u32[]{:S(2)}) copy-start(bf16[512,2048]{1,0:T(8,128)(2,1)} %param.37) | copy-start | bytes 6291460
  6.5 7.9 %copy-start.14 = (bf16[128,512]{1,0:T(8,128)(2,1)S(1)}, bf16[128,512]{1,0:T(8,128)(2,1)}, u32[]{:S(2)}) copy-start(bf16[128,512]{1,0:T(8,128)(2,1)} %param.25) | copy-start | bytes 393220
  6.5 65.9 %all-gather.18.cloned.1.call-start = ((), (), s32[]{:S(2)}) async-start(), calls=%async_computation.8 | async-start | bytes 1114112 | tf_op jit(solution)/shard_map/all_gather | solution.py:20
  10.4 4.4 copy-start.15
  14.4 135.2 %all-gather.16.cloned.1.call-start = ((), (), s32[]{:S(2)}) async-start(), calls=%async_computation.7 | async-start | bytes 4456448 | tf_op jit(solution)/shard_map/all_gather | solution.py:20
  16.3 3.5 copy-start.16
  16.9 3.1 copy-start.34
  18.0 48.8 %copy-start.11 = (bf16[128,1024]{1,0:T(8,128)(2,1)S(1)}, bf16[128,1024]{1,0:T(8,128)(2,1)}, u32[]{:S(2)}) copy-start(bf16[128,1024]{1,0:T(8,128)(2,1)} %param.31) | copy-start | bytes 786436
  18.0 49.6 %copy-start.32 = (bf16[1024]{0:T(1024)(128)(2,1)S(1)}, bf16[1024]{0:T(1024)(128)(2,1)}, u32[]{:S(2)}) copy-start(bf16[1024]{0:T(1024)(128)(2,1)} %param.34) | copy-start | bytes 6148
  18.0 50.2 %copy-start.33 = (bf16[512]{0:T(512)(128)(2,1)S(1)}, bf16[512]{0:T(512)(128)(2,1)}, u32[]{:S(2)}) copy-start(bf16[512]{0:T(512)(128)(2,1)} %param.35) | copy-start | bytes 3076
  18.0 50.8 %copy-start.4 = (bf16[128,512]{0,1:T(8,128)(2,1)S(1)}, bf16[128,512]{0,1:T(8,128)(2,1)}, u32[]{:S(2)}) copy-start(bf16[128,512]{0,1:T(8,128)(2,1)} %copy-done.3) | copy-start | bytes 393220
  18.0 50.8 %copy-start.5 = (bf16[128,4,32]{0,2,1:T(8,128)(2,1)S(1)}, bf16[128,4,32]{0,2,1:T(8,128)(2,1)}, u32[]{:S(2)}) copy-start(bf16[128,4,32]{0,2,1:T(8,128)(2,1)} %get-tuple-element.211) | copy-start | bytes 98308
  18.0 50.8 %copy-start.6 = (bf16[128,4,32]{0,2,1:T(8,128)(2,1)S(1)}, bf16[128,4,32]{0,2,1:T(8,128)(2,1)}, u32[]{:S(2)}) copy-start(bf16[128,4,32]{0,2,1:T(8,128)(2,1)} %get-tuple-element.212) | copy-start | bytes 98308
  18.0 50.8 %copy-start.8 = (f32[128,4,32]{0,2,1:T(8,128)S(1)}, f32[128,4,32]{0,2,1:T(8,128)}, u32[]{:S(2)}) copy-start(f32[128,4,32]{0,2,1:T(8,128)} %copy-done.7) | copy-start | bytes 196612
  18.0 50.8 %copy-start.10 = (f32[128,4,32]{0,2,1:T(8,128)S(1)}, f32[128,4,32]{0,2,1:T(8,128)}, u32[]{:S(2)}) copy-start(f32[128,4,32]{0,2,1:T(8,128)} %copy-done.9) | copy-start | bytes 196612
  18.1 50.8 %copy-start.21 = (f32[4,128]{1,0:T(4,128)S(1)}, f32[4,128]{1,0:T(4,128)}, u32[]{:S(2)}) copy-start(f32[4,128]{1,0:T(4,128)} %copy-done.20) | copy-start | bytes 6148
  19.9 189.9 %reduce-scatter.3.cloned.1.call-start = ((), (), s32[]{:S(2)}) async-start(), calls=%async_computation.2 | async-start | bytes 786432 | tf_op jit(solution)/shard_map/reduce_scatter | solution.py:206
  158.0 3.0 copy-start.2
  158.0 3.0 copy-start.13
  162.4 48.5 %copy-start.12 = (bf16[64,2048]{1,0:T(8,128)(2,1)S(1)}, bf16[64,2048]{1,0:T(8,128)(2,1)}, u32[]{:S(2)}) copy-start(bf16[64,2048]{1,0:T(8,128)(2,1)} %param.24) | copy-start | bytes 786436
  162.4 182.5 %all-gather.10.cloned.1.call-start = ((), (), s32[]{:S(2)}) async-start(), calls=%async_computation.3 | async-start | bytes 11141120 | tf_op jit(solution)/shard_map/all_gather | solution.py:213
  163.0 314.1 %all-gather.12.cloned.1.call-start = ((), (), s32[]{:S(2)}) async-start(), calls=%async_computation.4 | async-start | bytes 11141120 | tf_op jit(solution)/shard_map/all_gather | solution.py:214
  163.6 445.8 %all-gather.14.cloned.1.call-start = ((), (), s32[]{:S(2)}) async-start(), calls=%async_computation.5 | async-start | bytes 11141120 | tf_op jit(solution)/shard_map/all_gather | solution.py:229
  164.2 462.5 %reduce-scatter.5.cloned.1.call-start = ((), (), s32[]{:S(2)}) async-start(), calls=%async_computation.6 | async-start | bytes 786432 | tf_op jit(solution)/shard_map/reduce_scatter | solution.py:233
  351.1 135.0 %collective-permute-start = (bf16[2,2560]{1,0:T(2,128)(2,1)}, bf16[2,2560]{1,0:T(2,128)(2,1)}, u32[]{:S(2)}, u32[]{:S(2)}) collective-permute-start(bf16[2,2560]{1,0:T(2,128)(2,1)} %slice.114), channel_id=1, source_target_pairs={{0,2},{2,4},{4,6},{6,8},{8,10},{10,12},{12,14},{14,16},{16,18},{18... | collective-permute-start | bytes 30728 | tf_op jit(solution)/shard_map/ppermute | solution.py:42
  482.7 5.4 collective-permute-start.1
  488.1 121.3 %copy-start.23 = (f32[2560]{0:T(1024)S(1)}, f32[2560]{0:T(1024)}, u32[]{:S(2)}) copy-start(f32[2560]{0:T(1024)} %get-tuple-element.177) | copy-start | bytes 30724
  488.1 121.3 %copy-start.24 = (f32[2560]{0:T(1024)S(1)}, f32[2560]{0:T(1024)}, u32[]{:S(2)}) copy-start(f32[2560]{0:T(1024)} %get-tuple-element.178) | copy-start | bytes 30724
  488.1 121.3 %copy-start.25 = (f32[2560]{0:T(1024)S(1)}, f32[2560]{0:T(1024)}, u32[]{:S(2)}) copy-start(f32[2560]{0:T(1024)} %get-tuple-element.239) | copy-start | bytes 30724
  488.1 121.3 %copy-start.26 = (f32[2560]{0:T(1024)S(1)}, f32[2560]{0:T(1024)}, u32[]{:S(2)}) copy-start(f32[2560]{0:T(1024)} %get-tuple-element.240) | copy-start | bytes 30724
  488.1 121.3 %copy-start.27 = (f32[2560]{0:T(1024)S(1)}, f32[2560]{0:T(1024)}, u32[]{:S(2)}) copy-start(f32[2560]{0:T(1024)} %get-tuple-element.241) | copy-start | bytes 30724
  609.4 11.0 %copy-start.31 = (bf16[2048]{0:T(1024)(128)(2,1)S(1)}, bf16[2048]{0:T(1024)(128)(2,1)}, u32[]{:S(2)}) copy-start(bf16[2048]{0:T(1024)(128)(2,1)} %param.40) | copy-start | bytes 12292
  (12 other events, 19.5 us)
Sparse Core Ops, SparseCore 0:
  14.5 57.8 all-gather.17
  75.2 74.4 all-gather.15
  162.6 47.1 reduce-scatter.2
  212.3 132.5 all-gather.9
  347.5 129.6 all-gather.11
  479.7 129.6 all-gather.13
  620.5 6.0 reduce-scatter.4
where the time goes:
time: 638 us; the launch traced here: 636 us
  waiting for transfers between devices  503 us (79%)
  blocking collectives  45.9 us (7%)
  matrix products  35.7 us (6%)
  other arithmetic  18.7 us (3%)
  between operations  14.9 us (2%)
  local copies, waits for them, and re-layouts  11.2 us (2%)
  starting transfers between devices  7.52 us (1%)
    all_gather x1, waiting for transfers between devices, body(): lax.all_gather(weight_gate, 'sp', axis=0, tiled=True)  130 us
    all_gather x1, waiting for transfers between devices, body(): lax.all_gather(weight_lin, 'sp', axis=0, tiled=True)  122 us
    all_gather x1, waiting for transfers between devices, body(): lax.all_gather(weight_down, 'sp', axis=0, tiled=True)  120 us
    all_gather x2, waiting for transfers between devices, carried_in(): lax.all_gather(a.astype(kind), axis)  77.4 us
    reduce_scatter x1, waiting for transfers between devices, body(): lax.psum_scatter((part_wide + part_narrow).astype(jnp.bfloat16), 'tp', sc...  44.7 us
    unnamed x1, blocking collectives  43.7 us
  transfers between devices with their start and end apart: 9, of which 7 were waited for; matrix products, arithmetic and copies ran while one was open for 5% of the time, Pallas kernels for 0%

commit v1 on v0

--- a/solution.py
+++ b/solution.py
@@ -12,28 +12,6 @@
 
 EPS = 1e-06
 THETA = 10000.0
-
-
-def carried_in(x, axis, join, neutral):
-    place = lax.axis_index(axis)
-    gathered = jax.tree.map(
-        lambda a, kind: lax.all_gather(a.astype(kind), axis),
-        x,
-        (jnp.bfloat16, jnp.bfloat16, jnp.bfloat16, jnp.bfloat16),
-    )
-    state = jax.tree.map(lambda a, e: jnp.zeros_like(a) + jnp.asarray(e, a.dtype), x, neutral)
-
-    def one(lap, state):
-        return join(
-            state,
-            jax.tree.map(
-                lambda a, own: lax.dynamic_index_in_dim(a, lap, 0, False).astype(own.dtype),
-                gathered,
-                x,
-            ),
-        )
-
-    return lax.fori_loop(0, place, one, state)
 
 
 def passed_along(value, axis, steps):
@@ -141,13 +119,125 @@
     return smooth
 
 
-def chain(earlier, later):
-    return (
-        earlier[0] * later[2] + later[0],
-        earlier[1] * later[3] + later[1],
-        earlier[2] * later[2],
-        earlier[3] * later[3],
-    )
+def swap_blocks(blocks, axis):
+    return lax.all_to_all(blocks, axis, 0, 0, tiled=False)
+
+
+def share_rows(parts, axis):
+    count = lax.axis_size(axis)
+    place = lax.axis_index(axis)
+    total = lax.dynamic_index_in_dim(parts, place, 0, False).astype(jnp.float32)
+    for step in range(1, count):
+        piece = lax.dynamic_index_in_dim(parts, (place + step) % count, 0, False)
+        moved = lax.ppermute(piece, axis, [(i, (i + step) % count) for i in range(count)])
+        total = total + moved.astype(jnp.float32)
+    return total
+
+
+def carried_in(states, decays, axis):
+    count = lax.axis_size(axis)
+    place = lax.axis_index(axis)
+    lanes = states[-1].shape[-1]
+    flat = jnp.concatenate([s.reshape(-1, lanes) for s in states]).astype(jnp.bfloat16)
+    rates = jnp.concatenate(
+        [jnp.repeat(d, s.size // s.shape[0] // lanes) for s, d in zip(states, decays)]
+    )
+    share = flat.shape[0] // count
+    every = lax.all_gather(rates, axis)
+    mine = lax.dynamic_slice_in_dim(every, place * share, share, 1)
+    got = swap_blocks(flat.reshape(count, share, lanes), axis).astype(jnp.float32)
+    level = jnp.zeros((share, lanes), jnp.float32)
+    before = []
+    for step in range(count):
+        before.append(level.astype(jnp.bfloat16))
+        level = level * mine[step][:, None] + got[step]
+    back = swap_blocks(jnp.stack(before), axis).reshape(-1, lanes).astype(jnp.float32)
+    outs, at = [], 0
+    for s in states:
+        rows = s.size // lanes
+        outs.append(back[at : at + rows].reshape(s.shape))
+        at += rows
+    return outs
+
+
+def feed_by_weights(normed_in, weight_gate, weight_lin, weight_down, taps_gate, taps_lin):
+    normed_all = lax.all_gather(normed_in, "tp", axis=0, tiled=True)
+    rows = normed_all.shape[0]
+    whole_gate, whole_lin = (
+        lax.all_gather(weight_gate, "sp", axis=0, tiled=True),
+        lax.all_gather(weight_lin, "sp", axis=0, tiled=True),
+    )
+    up_gate = jnp.dot(normed_all, whole_gate, preferred_element_type=jnp.float32).astype(
+        jnp.bfloat16
+    )
+    up_lin = jnp.dot(normed_all, whole_lin, preferred_element_type=jnp.float32).astype(jnp.bfloat16)
+    reach = taps_gate.shape[0] - 1
+    before_gate, before_lin = passed_along(
+        (up_gate[rows - reach :], up_lin[rows - reach :]), "sp", 1
+    )
+    smooth_gate = causal_taps(up_gate, before_gate, taps_gate)
+    smooth_lin = causal_taps(up_lin, before_lin, taps_lin)
+    hidden = (jax.nn.silu(smooth_gate) * smooth_lin).astype(jnp.bfloat16)
+    terms = lax.dot_general(
+        hidden,
+        lax.all_gather(weight_down, "sp", axis=0, tiled=True),
+        (((1,), (1,)), ((), ())),
+        preferred_element_type=jnp.float32,
+    )
+    return lax.psum_scatter(
+        terms.astype(jnp.bfloat16), "tp", scatter_dimension=0, tiled=True
+    ).astype(jnp.float32)
+
+
+def from_all(value, axis, dim):
+    count = lax.axis_size(axis)
+    found = [value]
+    for step in range(1, count):
+        found.append(lax.ppermute(value, axis, [(i, (i + step) % count) for i in range(count)]))
+    return jnp.concatenate(found, axis=dim)
+
+
+def unit_slices(weight_gate, weight_lin, weight_down, taps_gate, taps_lin):
+    count = lax.axis_size("sp")
+    place = lax.axis_index("sp")
+    deep, units = weight_gate.shape
+    share = units // count
+    turned = jnp.stack([weight_gate.T, weight_lin.T, weight_down.T])
+    blocks = turned.reshape(3, count, share, deep).transpose(1, 0, 2, 3)
+    got = swap_blocks(blocks, "sp")
+    mine = got.transpose(1, 2, 0, 3).reshape(3, share, count * deep)
+    taps = jnp.stack([taps_gate, taps_lin])
+    taps = lax.dynamic_slice_in_dim(taps, place * share, share, 2)
+    return from_all(mine, "tp", 1), from_all(taps, "tp", 2)
+
+
+def feed_by_tokens(normed_in, weights, taps):
+    count = lax.axis_size("sp")
+    n_tp = lax.axis_size("tp")
+    rows, width = normed_in.shape
+    tokens = lax.all_gather(normed_in, "sp", axis=0, tiled=True)
+    flat = weights[:2].reshape(-1, width)
+    ups = lax.dot_general(
+        tokens, flat, (((1,), (1,)), ((), ())), preferred_element_type=jnp.float32
+    ).astype(jnp.bfloat16)
+    units = flat.shape[0] // 2
+    ups = ups.reshape(count, rows, 2 * units)
+    reach = taps.shape[1] - 1
+    tails = ups[:, rows - reach :]
+    prior = lax.ppermute(tails, "tp", [(i, (i + 1) % n_tp) for i in range(n_tp)])
+    prior = jnp.roll(prior.reshape(count, reach, 2, n_tp, -1), 1, axis=3).reshape(prior.shape)
+    shifted = jnp.concatenate([jnp.zeros_like(prior[:1]), prior[:-1]], axis=0)
+    prior = jnp.where(lax.axis_index("tp") == 0, shifted, prior)
+    padded = jnp.concatenate([prior, ups], axis=1).astype(jnp.float32)
+    taps = jnp.concatenate([taps[0], taps[1]], axis=1).astype(jnp.float32)
+    smooth = sum(taps[j] * padded[:, j : j + rows] for j in range(reach + 1))
+    hidden = (jax.nn.silu(smooth[..., :units]) * smooth[..., units:]).astype(jnp.bfloat16)
+    terms = jnp.dot(
+        hidden.reshape(count * rows, units), weights[2], preferred_element_type=jnp.float32
+    )
+    return lax.psum_scatter(
+        terms.astype(jnp.bfloat16), "sp", scatter_dimension=0, tiled=True
+    ).astype(jnp.float32)
 
 
 def body(
@@ -175,6 +265,13 @@
     taps_lin,
 ):
     rows = wide_head_query.shape[0]
+    count = lax.axis_size("sp")
+    n_tp = lax.axis_size("tp")
+    width = stream.shape[1]
+    units = weight_gate.shape[1]
+    by_tokens = 2 * count * rows < 3 * units and units % (count * 16) == 0
+    if by_tokens:
+        weights, taps = unit_slices(weight_gate, weight_lin, weight_down, taps_gate, taps_lin)
     offset = lax.axis_index("sp") * rows
     rates_wide = log_decay[0]
     rates_narrow = log_decay[1]
@@ -184,16 +281,10 @@
     rot_narrow, local_narrow, state_narrow = kept_nearby_memory(
         query_narrow, keys_narrow, values_narrow, rates_narrow, KN, VN, offset
     )
-    decay_wide = jnp.exp(jnp.sum(rates_wide, axis=1))[:, None, None]
-    decay_narrow = jnp.exp(jnp.sum(rates_narrow, axis=1))[:, None, None]
-    identity = (
-        jnp.zeros_like(state_wide),
-        jnp.zeros_like(state_narrow),
-        jnp.ones_like(decay_wide),
-        jnp.ones_like(decay_narrow),
-    )
     incoming = carried_in(
-        (state_wide, state_narrow, decay_wide, decay_narrow), "sp", chain, identity
+        (state_wide, state_narrow),
+        (jnp.exp(jnp.sum(rates_wide, axis=1)), jnp.exp(jnp.sum(rates_narrow, axis=1))),
+        "sp",
     )
     gated_wide = gate_heads(
         local_wide + carried(rot_wide, rates_wide, incoming[0]), gain_wide, gate_wide
@@ -203,36 +294,15 @@
     )
     part_wide = jnp.dot(gated_wide, out_wide, preferred_element_type=jnp.float32)
     part_narrow = jnp.dot(gated_narrow, out_narrow, preferred_element_type=jnp.float32)
-    mixed = lax.psum_scatter(
-        (part_wide + part_narrow).astype(jnp.bfloat16), "tp", scatter_dimension=0, tiled=True
-    ).astype(jnp.float32)
+    mixed = share_rows(
+        (part_wide + part_narrow).astype(jnp.bfloat16).reshape(n_tp, rows // n_tp, width), "tp"
+    )
     resid = (stream.astype(jnp.float32) + scale_rows(mixed, gain_mix)).astype(jnp.bfloat16)
     normed_in = scale_rows(resid.astype(jnp.float32), gain_pre).astype(jnp.bfloat16)
-    normed_all = lax.all_gather(normed_in, "tp", axis=0, tiled=True)
-    whole_gate, whole_lin = (
-        lax.all_gather(weight_gate, "sp", axis=0, tiled=True),
-        lax.all_gather(weight_lin, "sp", axis=0, tiled=True),
-    )
-    up_gate = jnp.dot(normed_all, whole_gate, preferred_element_type=jnp.float32).astype(
-        jnp.bfloat16
-    )
-    up_lin = jnp.dot(normed_all, whole_lin, preferred_element_type=jnp.float32).astype(jnp.bfloat16)
-    reach = taps_gate.shape[0] - 1
-    before_gate, before_lin = passed_along(
-        (up_gate[rows - reach :], up_lin[rows - reach :]), "sp", 1
-    )
-    smooth_gate = causal_taps(up_gate, before_gate, taps_gate)
-    smooth_lin = causal_taps(up_lin, before_lin, taps_lin)
-    hidden = (jax.nn.silu(smooth_gate) * smooth_lin).astype(jnp.bfloat16)
-    terms = lax.dot_general(
-        hidden,
-        lax.all_gather(weight_down, "sp", axis=0, tiled=True),
-        (((1,), (1,)), ((), ())),
-        preferred_element_type=jnp.float32,
-    )
-    fed = lax.psum_scatter(
-        terms.astype(jnp.bfloat16), "tp", scatter_dimension=0, tiled=True
-    ).astype(jnp.float32)
+    if by_tokens:
+        fed = feed_by_tokens(normed_in, weights, taps)
+    else:
+        fed = feed_by_weights(normed_in, weight_gate, weight_lin, weight_down, taps_gate, taps_lin)
     return (resid.astype(jnp.float32) + scale_rows(fed, gain_post)).astype(jnp.bfloat16)
 
 

time: 638 us -> 341 us (0.53)
  waiting for transfers between devices: 503 us -> 109 us
  blocking collectives: 45.9 us -> 111 us
  other arithmetic: 18.7 us -> 38.6 us
  local copies, waits for them, and re-layouts: 11.2 us -> 30.1 us
  matrix products: 35.7 us -> 23.4 us
    all_gather x5 -> x1, waiting for transfers between devices: 450 us -> 5.62 us  [feed_by_tokens(): tokens = lax.all_gather(normed_in, 'sp', axis=0, tiled=True)]
    all_to_all x0 -> x1, blocking collectives: none -> 69.6 us  [swap_blocks(): return lax.all_to_all(blocks, axis, 0, 0, tiled=False)]
    unnamed x1 -> x0, blocking collectives: 43.7 us -> none
    reduce_scatter x2 -> x1, waiting for transfers between devices: 51 us -> 93.3 us  [feed_by_tokens(): lax.psum_scatter(terms.astype(jnp.bfloat16), 'sp', scatter_dimension=0, t...]
    all_gather x1, blocking collectives: 2.18 us -> 41.4 us  [carried_in(): every = lax.all_gather(rates, axis)]
    unnamed x0 -> x14, other arithmetic: none -> 19.2 us
    all_to_all x0 -> x2, starting transfers between devices: none -> 11.9 us  [swap_blocks(): return lax.all_to_all(blocks, axis, 0, 0, tiled=False)]
    unnamed x84 -> x69, local copies, waits for them, and re-layouts: 7.09 us -> 18.8 us
  transfers between devices with their start and end apart: 9 -> 8, of which waited for: 7 -> 6; matrix products, arithmetic and copies ran while one was open for 5% -> 8% of each run, Pallas kernels for 0% -> 0%
where the time goes in v1:
time: 341 us; the launch traced here: 339 us
  blocking collectives  111 us (33%)
  waiting for transfers between devices  109 us (32%)
  other arithmetic  38.6 us (11%)
  local copies, waits for them, and re-layouts  30.1 us (9%)
  matrix products  23.4 us (7%)
  between operations  14.1 us (4%)
  starting transfers between devices  12.5 us (4%)
    reduce_scatter x1, waiting for transfers between devices, feed_by_tokens(): lax.psum_scatter(terms.astype(jnp.bfloat16), 'sp', scatter_dimension=0, t...  93.3 us
    all_to_all x1, blocking collectives, swap_blocks(): return lax.all_to_all(blocks, axis, 0, 0, tiled=False)  69.6 us
    all_gather x1, blocking collectives, carried_in(): every = lax.all_gather(rates, axis)  41.4 us
    unnamed x14, other arithmetic  19.2 us
    unnamed x69, local copies, waits for them, and re-layouts  18.8 us
    all_to_all x2, starting transfers between devices, swap_blocks(): return lax.all_to_all(blocks, axis, 0, 0, tiled=False)  11.9 us
  transfers between devices with their start and end apart: 8, of which 6 were waited for; matrix products, arithmetic and copies ran while one was open for 8% of the time, Pallas kernels for 0%

profile of v1, /device:TPU:0, one launch (start us, length us, event | category | flops | bytes accessed | tf_op | source)
XLA Modules:
  0.0 339.0 jit_solution(7835648636337791486)
XLA Ops:
  19.4 8.3 %all-to-all-start = ((bf16[16,80,128]{2,1,0:T(8,128)(2,1)}), bf16[16,80,128]{2,1,0:T(8,128)(2,1)S(1)}, u32[]{:S(2)}, u32[]{:S(2)}) async-start(bf16[16,80,128]{2,1,0:T(8,128)(2,1)} %bitcast.15), calls=%async_computation | async-start | bytes 655360 | tf_op jit(solution)/shard_map/all_to_all | solution.py:123
  28.0 1.8 copy.93
  31.0 41.4 %all-gather.1 = f32[16,1,1280]{2,1,0:T(1,128)S(1)} all-gather(f32[1,1,1280]{2,1,0:T(1,128)S(1)} %reshape.1017), channel_id=2, replica_groups=mesh['sp'=16,'tp'=2] {'sp'}, dimensions={0}, use_global_device_ids=true | all-gather | bytes 87040 | tf_op jit(solution)/shard_map/all_gather | solution.py:146
  74.7 1.5 constant_dynamic-update-slice_fusion.12
  76.2 1.5 constant_dynamic-update-slice_fusion.11
  77.6 1.5 constant_dynamic-update-slice_fusion.10
  79.1 1.5 constant_dynamic-update-slice_fusion.9
  80.6 1.5 constant_dynamic-update-slice_fusion.8
  82.1 1.5 constant_dynamic-update-slice_fusion.7
  85.0 1.5 constant_dynamic-update-slice_fusion.5
  86.5 1.5 constant_dynamic-update-slice_fusion.4
  88.0 1.5 constant_dynamic-update-slice_fusion.3
  89.5 1.5 constant_dynamic-update-slice_fusion.2
  90.9 1.5 constant_dynamic-update-slice_fusion.1
  92.4 1.5 constant_dynamic-update-slice_fusion
  93.9 3.5 %all-to-all-start.1 = ((bf16[16,80,128]{2,1,0:T(8,128)(2,1)}), bf16[16,80,128]{2,1,0:T(8,128)(2,1)S(1)}, u32[]{:S(2)}, u32[]{:S(2)}) async-start(bf16[16,80,128]{2,1,0:T(8,128)(2,1)} %constant_dynamic-update-slice_fusion), calls=%async_computation.1 | async-start | bytes 655360 | tf_op jit(solution)/shard_map/all_to_all | solution.py:123
  100.1 6.3 %all-to-all-done.1 = bf16[16,80,128]{2,1,0:T(8,128)(2,1)S(1)} async-done(((bf16[16,80,128]{2,1,0:T(8,128)(2,1)}), bf16[16,80,128]{2,1,0:T(8,128)(2,1)S(1)}, u32[]{:S(2)}, u32[]{:S(2)}) %all-to-all-start.1) | async-done | bytes 327712 | tf_op jit(solution)/shard_map/all_to_all | solution.py:123
  111.7 2.2 fusion.106
  115.6 3.0 fusion.108
  126.4 2.2 copy.99
  130.0 69.6 %all_to_all.15 = bf16[16,3,160,128]{3,2,1,0:T(8,128)(2,1)S(1)} all-to-all(bf16[16,3,160,128]{3,2,1,0:T(8,128)(2,1)S(1)} %copy.100), channel_id=1, replica_groups=mesh['sp'=16,'tp'=2] {'sp'}, dimensions={0} | all-to-all | bytes 3932160 | tf_op jit(solution)/shard_map/all_to_all | solution.py:123
  200.9 1.5 copy_bitcast_fusion
  203.1 1.8 constant_dynamic-update-slice_fusion.17
  204.9 1.9 collective-permute-done.2
  206.8 1.8 constant_dynamic-update-slice_fusion.16
  208.6 1.9 copy-done.2
  210.4 1.9 slice.332
  212.3 5.6 %all-gather.4.cloned.1.call-done = bf16[1024,2048]{1,0:T(8,128)(2,1)} async-done(((bf16[64,2048]{1,0:T(8,128)(2,1)}), bf16[1024,2048]{1,0:T(8,128)(2,1)}) %all-gather.4.cloned.1.call-update) | async-done | bytes 4194320 | tf_op jit(solution)/shard_map/all_gather | solution.py:218
  218.0 6.5 %convolution_convert_fusion.1 = bf16[1024,640]{1,0:T(8,128)(2,1)S(1)} fusion(bf16[1024,2048]{1,0:T(8,128)(2,1)} %all-gather.4.cloned.1.call-done, bf16[640,2048]{1,0:T(8,128)(2,1)} %bitcast.148), kind=kOutput, calls=%fused_computation.10 | convolution fusion | flops 2685009920 | bytes 8126464 | tf_op jit(solution)/shard_map/dot_general | solution.py:220
  229.7 5.6 %convolution_convert_fusion = bf16[1024,2048]{1,0:T(8,128)(2,1)} fusion(bf16[1024,320]{1,0:T(8,128)(2,1)S(1)} %bitcast.161, bf16[3,320,2048]{2,1,0:T(8,128)(2,1)} %copy-done.2), kind=kOutput, calls=%fused_computation | convolution fusion | flops 1344274432 | bytes 6160384 | tf_op jit(solution)/shard_map/dot_general | solution.py:235
  235.9 93.3 %reduce-scatter.2.cloned.1.call-done = bf16[64,2048]{1,0:T(8,128)(2,1)} async-done(((bf16[1024,2048]{1,0:T(8,128)(2,1)}), bf16[64,2048]{1,0:T(8,128)(2,1)}) %reduce-scatter.2.cloned.1.call-update) | async-done | bytes 262160 | tf_op jit(solution)/shard_map/reduce_scatter | solution.py:238
  330.3 1.8 fusion.21
  (161 shorter events, 45.4 us)
Async XLA Ops:
  6.5 112.0 %copy-start = (bf16[512,2048]{1,0:T(8,128)(2,1)S(1)}, bf16[512,2048]{1,0:T(8,128)(2,1)}, u32[]{:S(2)}) copy-start(bf16[512,2048]{1,0:T(8,128)(2,1)} %param.35) | copy-start | bytes 6291460
  6.5 4.3 %copy-start.22 = (f32[2,4,128]{2,1,0:T(4,128)S(1)}, f32[2,4,128]{2,1,0:T(4,128)}, u32[]{:S(2)}) copy-start(f32[2,4,128]{2,1,0:T(4,128)} %param.31) | copy-start | bytes 12292
  7.8 6.4 %copy-start.6 = (bf16[128,1024]{1,0:T(8,128)(2,1)S(1)}, bf16[128,1024]{1,0:T(8,128)(2,1)}, u32[]{:S(2)}) copy-start(bf16[128,1024]{1,0:T(8,128)(2,1)} %param.25) | copy-start | bytes 786436
  11.7 2.5 copy-start.13
  14.0 13.7 %copy-start.25 = (f32[4]{0:T(128)S(1)}, f32[4]{0:T(128)}, u32[]{:S(2)}) copy-start(f32[4]{0:T(128)} %get-tuple-element.34) | copy-start | bytes 52
  14.2 15.7 %copy-start.23 = (bf16[1024]{0:T(1024)(128)(2,1)S(1)}, bf16[1024]{0:T(1024)(128)(2,1)}, u32[]{:S(2)}) copy-start(bf16[1024]{0:T(1024)(128)(2,1)} %param.32) | copy-start | bytes 6148
  14.2 16.2 %copy-start.24 = (bf16[512]{0:T(512)(128)(2,1)S(1)}, bf16[512]{0:T(512)(128)(2,1)}, u32[]{:S(2)}) copy-start(bf16[512]{0:T(512)(128)(2,1)} %param.33) | copy-start | bytes 3076
  17.3 80.6 %copy-start.17 = (f32[128,4]{0,1:T(4,128)}, f32[128,4]{0,1:T(4,128)S(1)}, u32[]{:S(2)}) copy-start(f32[128,4]{0,1:T(4,128)S(1)} %get-tuple-element.109) | copy-start | bytes 6148
  18.4 79.5 %copy-start.10 = (bf16[128,4,32]{0,2,1:T(8,128)(2,1)}, bf16[128,4,32]{0,2,1:T(8,128)(2,1)S(1)}, u32[]{:S(2)}) copy-start(bf16[128,4,32]{0,2,1:T(8,128)(2,1)S(1)} %get-tuple-element.76) | copy-start | bytes 98308
  18.4 79.5 %copy-start.11 = (bf16[128,4,32]{0,2,1:T(8,128)(2,1)}, bf16[128,4,32]{0,2,1:T(8,128)(2,1)S(1)}, u32[]{:S(2)}) copy-start(bf16[128,4,32]{0,2,1:T(8,128)(2,1)S(1)} %get-tuple-element.77) | copy-start | bytes 98308
  19.4 53.7 %all-to-all-start = ((bf16[16,80,128]{2,1,0:T(8,128)(2,1)}), bf16[16,80,128]{2,1,0:T(8,128)(2,1)S(1)}, u32[]{:S(2)}, u32[]{:S(2)}) async-start(bf16[16,80,128]{2,1,0:T(8,128)(2,1)} %bitcast.15), calls=%async_computation | async-start | bytes 655360 | tf_op jit(solution)/shard_map/all_to_all | solution.py:123
  73.2 1.5 copy-start.3
  93.9 12.5 %all-to-all-start.1 = ((bf16[16,80,128]{2,1,0:T(8,128)(2,1)}), bf16[16,80,128]{2,1,0:T(8,128)(2,1)S(1)}, u32[]{:S(2)}, u32[]{:S(2)}) async-start(bf16[16,80,128]{2,1,0:T(8,128)(2,1)} %constant_dynamic-update-slice_fusion), calls=%async_computation.1 | async-start | bytes 655360 | tf_op jit(solution)/shard_map/all_to_all | solution.py:123
  97.4 120.5 %all-gather.4.cloned.1.call-start = ((), (), s32[]{:S(2)}) async-start(), calls=%async_computation.4 | async-start | bytes 4456448 | tf_op jit(solution)/shard_map/all_gather | solution.py:218
  97.9 12.6 %copy-start.16 = (f32[128,4]{0,1:T(4,128)S(1)}, f32[128,4]{0,1:T(4,128)}, u32[]{:S(2)}) copy-start(f32[128,4]{0,1:T(4,128)} %get-tuple-element.111) | copy-start | bytes 6148
  113.9 1.4 copy-start.8
  113.9 1.4 copy-start.18
  115.5 3.0 copy-start.7
  115.5 3.0 copy-start.12
  115.6 3.0 copy-start.19
  118.6 1.3 copy-start.20
  118.6 6.1 %copy-start.9 = (bf16[128,2560]{1,0:T(8,128)(2,1)S(1)}, bf16[128,2560]{1,0:T(8,128)(2,1)}, u32[]{:S(2)}) copy-start(bf16[128,2560]{1,0:T(8,128)(2,1)} %param.39) | copy-start | bytes 1966084
  119.9 1.7 collective-permute-start
  124.6 204.6 %reduce-scatter.2.cloned.1.call-start = ((), (), s32[]{:S(2)}) async-start(), calls=%async_computation.5 | async-start | bytes 4456448 | tf_op jit(solution)/shard_map/reduce_scatter | solution.py:238
  199.6 1.3 copy-start.1
  200.9 1.6 copy-start.14
  200.9 1.6 copy-start.15
  202.5 4.3 %collective-permute-start.2 = (bf16[3,160,2048]{2,1,0:T(8,128)(2,1)}, bf16[3,160,2048]{2,1,0:T(8,128)(2,1)}, u32[]{:S(2)}, u32[]{:S(2)}) collective-permute-start(bf16[3,160,2048]{2,1,0:T(8,128)(2,1)} %copy_bitcast_fusion), channel_id=1, source_target_pairs={{0,1},{1,0},{2,3},{3,2},{4,5},{5,4},{6,7},{7,6},{8,9},{9,8},{10,11... | collective-permute-start | bytes 5898248 | tf_op jit(solution)/shard_map/ppermute | solution.py:196
  202.6 22.0 %collective-permute-start.1 = (bf16[2,3,160]{2,1,0:T(4,128)(2,1)S(1)}, bf16[2,3,160]{2,1,0:T(4,128)(2,1)S(1)}, u32[]{:S(2)}, u32[]{:S(2)}) collective-permute-start(bf16[2,3,160]{2,1,0:T(4,128)(2,1)S(1)} %fusion.63), channel_id=1, source_target_pairs={{0,1},{1,0},{2,3},{3,2},{4,5},{5,4},{6,7},{7,6},{8,9},{9,8},{10,11... | collective-permute-start | bytes 5768 | tf_op jit(solution)/shard_map/ppermute | solution.py:196
  208.6 1.9 copy-start.2
  224.5 1.3 collective-permute-start.3
  235.2 95.1 %copy-start.5 = (bf16[64,2048]{1,0:T(8,128)(2,1)S(1)}, bf16[64,2048]{1,0:T(8,128)(2,1)}, u32[]{:S(2)}) copy-start(bf16[64,2048]{1,0:T(8,128)(2,1)} %copy-done.4) | copy-start | bytes 786436
  (2 other events, 1.4 us)
Sparse Core Ops, SparseCore 0:
  124.7 93.1 all-gather.3
  235.4 93.7 reduce-scatter.1
